TPU v7x, 512 devices: a whole 4x8x8 slice. The times are simulated.
512 devices in a mesh: kv: 64 (over z, y), tp: 8 (over x, core).
Axes of the slice: x: 4, y: 8, z: 8, core: 2. Of those that a mesh axis runs over, the one named last changes fastest.
Arguments:
- tokens: bfloat16 [8, 8192, 2048], P(None, 'kv'), may hold values from -32 to 32, as said below
- w_query: bfloat16 [2048, 1024], P(None, 'tp'), may hold values from -0.125 to 0.125
- w_key: bfloat16 [2048, 512], P(None, 'tp'), may hold values from -0.125 to 0.125
- w_value: bfloat16 [2048, 512], P(None, 'tp'), may hold values from -0.125 to 0.125
- w_output: bfloat16 [1024, 2048], P(None, 'tp'), may hold values from -3 to 3
- chosen: int32 [8, 64, 32], P(None, 'kv'), may hold values from -1 to 63, as said below
- lengths: int32 [8], replicated, may hold values from 1 to 8192, 22528 in all
Outputs:
- mixed: bfloat16 [8, 8192, 2048], P(None, 'kv', 'tp')
Inputs may be any that keep to these rules, and one draw needn't show every extreme that they name: chosen[s, b] lists distinct blocks of sequence s, none above b; its first entry is b; entries after the named ones are -1. For b >= 1 and each c < b, at most 4 of the 8 lists chosen[:, b] name block c, and exactly 4 of them name block b - 1. lengths[s] is the number of live positions of sequence s; the largest is 8192. `tokens`: activations of order one; some rows may be much larger.
All inputs are finite; a program needn't handle non-finite values.
Results may differ from a plain program's by a relative error of at most 0.012.
The roundings to bfloat16 on the way count: a program that leaves them out, or rounds other values in their place, can miss the bound.
Values may be sent and summed in bfloat16 or wider, within the bound.
A program may use at most 128 MiB of HBM per device.

v0:
```python
import jax
import jax.numpy as jnp
from jax import lax
from jax.sharding import PartitionSpec as P

HEADS = 16
KV_HEADS = 8
HEAD_DIM = 64


def per_device(tokens, w_query, w_key, w_value, w_output, chosen, lengths):
    seq_count, block_len, model_width = tokens.shape
    flat_rows = tokens.reshape(seq_count * block_len, model_width)
    queries = jnp.dot(flat_rows, w_query, preferred_element_type=jnp.float32).astype(jnp.bfloat16)
    key_proj = jnp.dot(flat_rows, w_key, preferred_element_type=jnp.float32).astype(jnp.bfloat16)
    value_proj = jnp.dot(flat_rows, w_value, preferred_element_type=jnp.float32).astype(
        jnp.bfloat16
    )
    key_width = key_proj.shape[1]
    local_blocks = jnp.concatenate([key_proj, value_proj], axis=1).reshape(
        seq_count, block_len, 2 * key_width
    )
    shard_member = lax.axis_index("kv")
    kv_devices = lax.axis_size("kv")
    picked = chosen[:, 0, :]
    clipped = jnp.maximum(picked, 0)
    seq_index = jnp.arange(seq_count, dtype=jnp.int32)
    gathered = lax.all_gather(local_blocks, "kv", axis=1, tiled=True)
    key_lookup = gathered.reshape(seq_count * kv_devices, block_len, 2 * key_width)
    source = seq_index[:, None] * kv_devices + clipped
    group_size = HEADS // KV_HEADS
    local_kv_heads = key_width // HEAD_DIM
    query_pos = shard_member * block_len + jnp.arange(block_len, dtype=jnp.int32)
    score_scale = HEAD_DIM ** (-0.5)

    def attend(packed):
        query_rows, source_row, pick_row, length = packed
        fetched = key_lookup[source_row]
        slot_count = pick_row.shape[0]
        key_rows = fetched[:, :, :key_width].reshape(
            slot_count * block_len, local_kv_heads, HEAD_DIM
        )
        value_rows = fetched[:, :, key_width:].reshape(
            slot_count * block_len, local_kv_heads, HEAD_DIM
        )
        grouped = query_rows.reshape(block_len, local_kv_heads, group_size, HEAD_DIM)
        scores = (
            jnp.einsum("qkgd,nkd->kgqn", grouped, key_rows, preferred_element_type=jnp.float32)
            * score_scale
        )
        key_pos = (
            pick_row[:, None] * block_len + jnp.arange(block_len, dtype=jnp.int32)[None, :]
        ).reshape(-1)
        listed = jnp.repeat(pick_row >= 0, block_len)
        allowed = (
            listed[None, :] & (key_pos[None, :] <= query_pos[:, None]) & (key_pos[None, :] < length)
        )
        masked = jnp.where(allowed, scores, -1e30)
        row_max = jnp.max(masked, axis=-1, keepdims=True)
        exponent = jnp.exp(masked - row_max)
        weights = (exponent / jnp.sum(exponent, axis=-1, keepdims=True)).astype(jnp.bfloat16)
        mixed_heads = jnp.einsum(
            "kgqn,nkd->qkgd", weights, value_rows, preferred_element_type=jnp.float32
        )
        live_rows = (query_pos < length)[:, None, None, None]
        return jnp.where(live_rows, mixed_heads, 0.0).astype(jnp.bfloat16).reshape(block_len, -1)

    attended = lax.map(attend, (queries.reshape(seq_count, block_len, -1), source, picked, lengths))
    attended_rows = attended.reshape(seq_count * block_len, -1)
    summed = jnp.dot(
        lax.all_gather(attended_rows, "tp", axis=1, tiled=True),
        w_output,
        preferred_element_type=jnp.float32,
    )
    return summed.astype(jnp.bfloat16).reshape(seq_count, block_len, -1)


def solution(mesh):
    return jax.shard_map(
        per_device,
        mesh=mesh,
        in_specs=(
            P(None, "kv", None),
            P(None, "tp"),
            P(None, "tp"),
            P(None, "tp"),
            P(None, "tp"),
            P(None, "kv", None),
            P(),
        ),
        out_specs=P(None, "kv", "tp"),
        check_vma=False,
    )
```

profile of v0, /device:TPU:1, one launch (start us, length us, event | category | flops | bytes accessed | tf_op | source)
XLA Modules:
  0.0 374.0 jit_solution(2250813190140114071)
XLA Ops:
  6.5 3.8 %convolution_convert_fusion.2 = bf16[1024,64]{0,1:T(8,128)(2,1)S(1)} fusion(bf16[1024,2048]{1,0:T(8,128)(2,1)} %bitcast.109, bf16[2048,64]{0,1:T(8,128)(2,1)} %param.12), kind=kOutput, calls=%fused_computation.31 | convolution fusion | flops 268500992 | bytes 4587520 | tf_op jit(solution)/shard_map/dot_general | solution.py:16
  12.7 4.2 %convolution_convert_fusion.1 = bf16[1024,128]{1,0:T(8,128)(2,1)} fusion(bf16[1024,2048]{1,0:T(8,128)(2,1)} %bitcast.110, bf16[2048,128]{1,0:T(8,128)(2,1)S(1)} %copy-done.5), kind=kOutput, calls=%fused_computation.30 | convolution fusion | flops 537001984 | bytes 4980736 | tf_op jit(solution)/shard_map/dot_general | solution.py:14
  16.9 144.8 %all-gather.3.cloned.1.call-done = bf16[8,8192,128]{1,0,2:T(8,128)(2,1)} async-done(((bf16[8,128,128]{1,0,2:T(8,128)(2,1)}), bf16[8,8192,128]{1,0,2:T(8,128)(2,1)}) %all-gather.3.cloned.1.call-update) | async-done | bytes 16777232 | tf_op jit(solution)/shard_map/all_gather | solution.py:28
  161.7 23.5 %copy.16 = bf16[8,8192,128]{2,1,0:T(8,128)(2,1)} copy(bf16[8,8192,128]{1,0,2:T(8,128)(2,1)} %all-gather.3.cloned.1.call-done) | data formatting | bytes 33554432 | tf_op jit(solution)/shard_map/all_gather | solution.py:28
  185.2 145.3 %while.11 = (s32[]{:T(128)}, bf16[8,128,128]{2,1,0:T(8,128)(2,1)S(1)}, s32[8]{0:T(128)S(1)}, s32[8,32]{1,0:T(8,128)S(1)}, bf16[512,128,128]{2,1,0:T(8,128)(2,1)}...) while((s32[]{:T(128)}, bf16[8,128,128]{2,1,0:T(8,128)(2,1)S(1)}, ...), condition=%wide.region_3.4_spmd.clone, body=%wide.region_0.3_spmd.clone.sunk | while | flops 278443040 | bytes 19263052 | solution.py:68
  186.7 3.5 and_and_fusion.2
  190.2 6.5 %gather_fusion = bf16[32,128,128]{2,1,0:T(8,128)(2,1)S(1)} fusion(bf16[512,128,128]{2,1,0:T(8,128)(2,1)} %get-tuple-element.182, s32[1024]{0:T(1024)S(1)} %pad_clamp_fusion.2), kind=kCustom, calls=%fused_computation.clone.clone.1 | custom fusion | bytes 2097280 | tf_op jit(solution)/shard_map/while/body/eval_jaxpr/gather | solution.py:38
  204.9 3.5 and_and_fusion.2
  208.4 6.5 %gather_fusion = bf16[32,128,128]{2,1,0:T(8,128)(2,1)S(1)} fusion(bf16[512,128,128]{2,1,0:T(8,128)(2,1)} %get-tuple-element.182, s32[1024]{0:T(1024)S(1)} %pad_clamp_fusion.2), kind=kCustom, calls=%fused_computation.clone.clone.1 | custom fusion | bytes 2097280 | tf_op jit(solution)/shard_map/while/body/eval_jaxpr/gather | solution.py:38
  223.0 3.5 and_and_fusion.2
  226.6 6.5 %gather_fusion = bf16[32,128,128]{2,1,0:T(8,128)(2,1)S(1)} fusion(bf16[512,128,128]{2,1,0:T(8,128)(2,1)} %get-tuple-element.182, s32[1024]{0:T(1024)S(1)} %pad_clamp_fusion.2), kind=kCustom, calls=%fused_computation.clone.clone.1 | custom fusion | bytes 2097280 | tf_op jit(solution)/shard_map/while/body/eval_jaxpr/gather | solution.py:38
  241.2 3.5 and_and_fusion.2
  244.7 6.5 %gather_fusion = bf16[32,128,128]{2,1,0:T(8,128)(2,1)S(1)} fusion(bf16[512,128,128]{2,1,0:T(8,128)(2,1)} %get-tuple-element.182, s32[1024]{0:T(1024)S(1)} %pad_clamp_fusion.2), kind=kCustom, calls=%fused_computation.clone.clone.1 | custom fusion | bytes 2097280 | tf_op jit(solution)/shard_map/while/body/eval_jaxpr/gather | solution.py:38
  253.6 2.1 fusion.46
  259.4 3.5 and_and_fusion.2
  262.9 6.5 %gather_fusion = bf16[32,128,128]{2,1,0:T(8,128)(2,1)S(1)} fusion(bf16[512,128,128]{2,1,0:T(8,128)(2,1)} %get-tuple-element.182, s32[1024]{0:T(1024)S(1)} %pad_clamp_fusion.2), kind=kCustom, calls=%fused_computation.clone.clone.1 | custom fusion | bytes 2097280 | tf_op jit(solution)/shard_map/while/body/eval_jaxpr/gather | solution.py:38
  277.5 3.5 and_and_fusion.2
  281.1 6.5 %gather_fusion = bf16[32,128,128]{2,1,0:T(8,128)(2,1)S(1)} fusion(bf16[512,128,128]{2,1,0:T(8,128)(2,1)} %get-tuple-element.182, s32[1024]{0:T(1024)S(1)} %pad_clamp_fusion.2), kind=kCustom, calls=%fused_computation.clone.clone.1 | custom fusion | bytes 2097280 | tf_op jit(solution)/shard_map/while/body/eval_jaxpr/gather | solution.py:38
  295.7 3.5 and_and_fusion.2
  299.2 6.5 %gather_fusion = bf16[32,128,128]{2,1,0:T(8,128)(2,1)S(1)} fusion(bf16[512,128,128]{2,1,0:T(8,128)(2,1)} %get-tuple-element.182, s32[1024]{0:T(1024)S(1)} %pad_clamp_fusion.2), kind=kCustom, calls=%fused_computation.clone.clone.1 | custom fusion | bytes 2097280 | tf_op jit(solution)/shard_map/while/body/eval_jaxpr/gather | solution.py:38
  313.9 3.5 and_and_fusion.2
  317.4 6.5 %gather_fusion = bf16[32,128,128]{2,1,0:T(8,128)(2,1)S(1)} fusion(bf16[512,128,128]{2,1,0:T(8,128)(2,1)} %get-tuple-element.182, s32[1024]{0:T(1024)S(1)} %pad_clamp_fusion.2), kind=kCustom, calls=%fused_computation.clone.clone.1 | custom fusion | bytes 2097280 | tf_op jit(solution)/shard_map/while/body/eval_jaxpr/gather | solution.py:38
  331.3 32.8 %all-gather.5.cloned.1.call-done = bf16[1024,1024]{1,0:T(8,128)(2,1)} async-done(((bf16[1024,128]{1,0:T(8,128)(2,1)}), bf16[1024,1024]{1,0:T(8,128)(2,1)}) %all-gather.5.cloned.1.call-update) | async-done | bytes 2097168 | tf_op jit(solution)/shard_map/all_gather | solution.py:71
  364.1 3.1 convolution_convert_fusion
  (167 shorter events, 65.7 us)
Async XLA Ops:
  6.5 357.5 %copy-start = (bf16[1024,256]{1,0:T(8,128)(2,1)S(1)}, bf16[1024,256]{1,0:T(8,128)(2,1)}, u32[]{:S(2)}) copy-start(bf16[1024,256]{1,0:T(8,128)(2,1)} %param.13) | copy-start | bytes 1572868
  6.5 3.8 %copy-start.2 = (bf16[2048,64]{0,1:T(8,128)(2,1)S(1)}, bf16[2048,64]{0,1:T(8,128)(2,1)}, u32[]{:S(2)}) copy-start(bf16[2048,64]{0,1:T(8,128)(2,1)} %param.11) | copy-start | bytes 786436
  6.5 155.2 %all-gather.3.cloned.1.call-start = ((), (), s32[]{:S(2)}) async-start(), calls=%async_computation | async-start | bytes 17039360 | tf_op jit(solution)/shard_map/all_gather | solution.py:28
  6.5 3.8 %copy-start.1 = (bf16[8,128,2048]{2,1,0:T(8,128)(2,1)S(1)}, bf16[8,128,2048]{2,1,0:T(8,128)(2,1)}, u32[]{:S(2)}) copy-start(bf16[8,128,2048]{2,1,0:T(8,128)(2,1)} %param.9) | copy-start | bytes 12582916
  10.3 2.3 copy-start.4
  10.3 2.4 copy-start.5
  12.5 351.5 %all-gather.5.cloned.1.call-start = ((), (), s32[]{:S(2)}) async-start(), calls=%async_computation.1 | async-start | bytes 2359296 | tf_op jit(solution)/shard_map/all_gather | solution.py:71
  16.9 168.4 %copy-start.6 = (s32[8]{0:T(128)S(1)}, s32[8]{0:T(128)}, u32[]{:S(2)}) copy-start(s32[8]{0:T(128)} %param.15) | copy-start | bytes 100
  330.6 0.7 copy-start.3
Sparse Core Ops, SparseCore 0:
  12.7 148.9 all-gather.2
  331.4 32.6 all-gather.4
where the time goes:
time: 376 us; the launch traced here: 374 us
  waiting for transfers between devices  178 us (47%)
  local copies, waits for them, and re-layouts  102 us (27%)
  other arithmetic  44.2 us (12%)
  matrix products  36 us (10%)
  between operations  13.5 us (4%)
    all_gather x1, waiting for transfers between devices, per_device(): gathered = lax.all_gather(local_blocks, 'kv', axis=1, tiled=True)  145 us
    gather x8, local copies, waits for them, and re-layouts, attend(): fetched = key_lookup[source_row]  52.1 us
    all_gather x1, waiting for transfers between devices, per_device(): lax.all_gather(attended_rows, 'tp', axis=1, tiled=True)  32.8 us
    and x8, other arithmetic, attend(): listed[None, :] & (key_pos[None, :] <= query_pos[:, None])  27.7 us
    all_gather x1, local copies, waits for them, and re-layouts, per_device(): gathered = lax.all_gather(local_blocks, 'kv', axis=1, tiled=True)  23.5 us
    dot_general x8, matrix products, attend(): jnp.einsum('qkgd,nkd->kgqn', grouped, key_rows, preferred_element_type=jn...  16.5 us
    dynamic_slice x24, local copies, waits for them, and re-layouts, per_device(): lax.map(attend, (queries.reshape(seq_count, block_len, -1), source, picke...  11.7 us
    slice x8, local copies, waits for them, and re-layouts, attend(): fetched[:, :, :key_width]  11.5 us
  transfers between devices with their start and end apart: 2, of which 2 were waited for; matrix products, arithmetic and copies ran while one was open for 1% of the time, Pallas kernels for 0%

commit v1 on v0

--- a/solution.py
+++ b/solution.py
@@ -6,6 +6,11 @@
 HEADS = 16
 KV_HEADS = 8
 HEAD_DIM = 64
+
+
+def gather_from_all(x, axis, dim):
+    copies = jnp.concatenate([x] * lax.axis_size(axis), axis=dim)
+    return lax.all_to_all(copies, axis, dim, dim, tiled=True)
 
 
 def per_device(tokens, w_query, w_key, w_value, w_output, chosen, lengths):
@@ -25,7 +30,7 @@
     picked = chosen[:, 0, :]
     clipped = jnp.maximum(picked, 0)
     seq_index = jnp.arange(seq_count, dtype=jnp.int32)
-    gathered = lax.all_gather(local_blocks, "kv", axis=1, tiled=True)
+    gathered = gather_from_all(local_blocks, "kv", 1)
     key_lookup = gathered.reshape(seq_count * kv_devices, block_len, 2 * key_width)
     source = seq_index[:, None] * kv_devices + clipped
     group_size = HEADS // KV_HEADS

time: 376 us -> 935 us (2.49)
  waiting for transfers between devices: 178 us -> 680 us
  local copies, waits for them, and re-layouts: 102 us -> 139 us
  starting transfers between devices: 0.04 us -> 17.6 us
    all_to_all x0 -> x1, waiting for transfers between devices: none -> 559 us  [gather_from_all(): return lax.all_to_all(copies, axis, dim, dim, tiled=True)]
    all_gather x1 -> x0, waiting for transfers between devices: 145 us -> none  [per_device(): gathered = lax.all_gather(local_blocks, 'kv', axis=1, tiled=True)]
    all_gather x1, waiting for transfers between devices: 32.8 us -> 121 us  [per_device(): lax.all_gather(attended_rows, 'tp', axis=1, tiled=True)]
    unnamed x15 -> x74, local copies, waits for them, and re-layouts: 1.48 us -> 46 us
    all_gather x1 -> x0, local copies, waits for them, and re-layouts: 23.5 us -> none  [per_device(): gathered = lax.all_gather(local_blocks, 'kv', axis=1, tiled=True)]
    all_to_all x0 -> x1, starting transfers between devices: none -> 17.5 us  [gather_from_all(): return lax.all_to_all(copies, axis, dim, dim, tiled=True)]
    all_to_all x0 -> x1, local copies, waits for them, and re-layouts: none -> 15.1 us  [gather_from_all(): return lax.all_to_all(copies, axis, dim, dim, tiled=True)]
  transfers between devices with their start and end apart: 2 -> 2, of which waited for: 2 -> 2; matrix products, arithmetic and copies ran while one was open for 1% -> 0% of each run, Pallas kernels for 0% -> 0%
where the time goes in v1:
time: 935 us; the launch traced here: 933 us
  waiting for transfers between devices  680 us (73%)
  local copies, waits for them, and re-layouts  139 us (15%)
  other arithmetic  43.9 us (5%)
  matrix products  38.1 us (4%)
  starting transfers between devices  17.6 us (2%)
  between operations  13.5 us (1%)
    all_to_all x1, waiting for transfers between devices, gather_from_all(): return lax.all_to_all(copies, axis, dim, dim, tiled=True)  559 us
    all_gather x1, waiting for transfers between devices, per_device(): lax.all_gather(attended_rows, 'tp', axis=1, tiled=True)  121 us
    gather x8, local copies, waits for them, and re-layouts, attend(): fetched = key_lookup[source_row]  52.1 us
    unnamed x74, local copies, waits for them, and re-layouts  46 us
    and x8, other arithmetic, attend(): listed[None, :] & (key_pos[None, :] <= query_pos[:, None])  27.7 us
  transfers between devices with their start and end apart: 2, of which 2 were waited for; matrix products, arithmetic and copies ran while one was open for 0% of the time, Pallas kernels for 0%

profile of v1, /device:TPU:1, one launch (start us, length us, event | category | flops | bytes accessed | tf_op | source)
XLA Modules:
  0.0 933.3 jit_solution(9824947096596880113)
XLA Ops:
  6.5 3.7 convolution_convert_fusion.2
  10.2 3.6 convolution_convert_fusion.3
  60.2 17.5 %all-to-all-start = ((bf16[8,8192,128]{2,0,1:T(8,128)(2,1)}), bf16[8,8192,128]{2,0,1:T(8,128)(2,1)}, u32[]{:S(2)}, u32[]{:S(2)}) async-start(bf16[8,8192,128]{2,0,1:T(8,128)(2,1)} %constant_dynamic-update-slice_fusion.1), calls=%async_computation | async-start | bytes 33554432 | tf_op jit(solution)/shard_map/all_to_all | solution.py:13
  77.8 4.1 convolution_convert_fusion.1
  82.0 559.3 %all-to-all-done = bf16[8,8192,128]{2,0,1:T(8,128)(2,1)} async-done(((bf16[8,8192,128]{2,0,1:T(8,128)(2,1)}), bf16[8,8192,128]{2,0,1:T(8,128)(2,1)}, u32[]{:S(2)}, u32[]{:S(2)}) %all-to-all-start) | async-done | bytes 16777248 | tf_op jit(solution)/shard_map/all_to_all | solution.py:13
  641.3 15.1 %copy.296 = bf16[8,8192,128]{2,1,0:T(8,128)(2,1)} copy(bf16[8,8192,128]{2,0,1:T(8,128)(2,1)} %all-to-all-done) | data formatting | bytes 33554432 | tf_op jit(solution)/shard_map/all_to_all | solution.py:13
  656.3 145.1 %while.11 = (s32[]{:T(128)}, bf16[8,128,128]{2,1,0:T(8,128)(2,1)S(1)}, s32[8]{0:T(128)S(1)}, s32[8,32]{1,0:T(8,128)S(1)}, bf16[512,128,128]{2,1,0:T(8,128)(2,1)}...) while((s32[]{:T(128)}, bf16[8,128,128]{2,1,0:T(8,128)(2,1)S(1)}, ...), condition=%wide.region_3.4_spmd.clone, body=%wide.region_0.3_spmd.clone.sunk | while | flops 278443040 | bytes 19263052 | solution.py:73
  657.8 3.5 and_and_fusion.2
  661.3 6.5 gather_fusion
  675.9 3.5 and_and_fusion.2
  679.4 6.5 gather_fusion
  694.1 3.5 and_and_fusion.2
  697.6 6.5 gather_fusion
  712.2 3.5 and_and_fusion.2
  715.7 6.5 gather_fusion
  730.4 3.5 and_and_fusion.2
  733.9 6.5 gather_fusion
  748.5 3.5 and_and_fusion.2
  752.0 6.5 gather_fusion
  766.6 3.5 and_and_fusion.2
  770.1 6.5 gather_fusion
  784.8 3.5 and_and_fusion.2
  788.3 6.5 gather_fusion
  802.1 121.2 %all-gather.2.cloned.1.call-done = bf16[1024,1024]{1,0:T(8,128)(2,1)} async-done(((bf16[1024,128]{1,0:T(8,128)(2,1)}), bf16[1024,1024]{1,0:T(8,128)(2,1)}) %all-gather.2.cloned.1.call-update) | async-done | bytes 2097168 | tf_op jit(solution)/shard_map/all_gather | solution.py:76
  (227 shorter events, 114.8 us)
Async XLA Ops:
  6.5 916.8 %copy-start = (bf16[1024,256]{1,0:T(8,128)(2,1)S(1)}, bf16[1024,256]{1,0:T(8,128)(2,1)}, u32[]{:S(2)}) copy-start(bf16[1024,256]{1,0:T(8,128)(2,1)} %param.13) | copy-start | bytes 1572868
  60.1 17.6 %copy-start.2 = (s32[8,1,32]{2,1,0:T(1,128)S(1)}, s32[8,1,32]{2,1,0:T(1,128)}, u32[]{:S(2)}) copy-start(s32[8,1,32]{2,1,0:T(1,128)} %param.14) | copy-start | bytes 3076
  60.1 17.7 %copy-start.3 = (bf16[2048,128]{1,0:T(8,128)(2,1)S(1)}, bf16[2048,128]{1,0:T(8,128)(2,1)}, u32[]{:S(2)}) copy-start(bf16[2048,128]{1,0:T(8,128)(2,1)} %param.10) | copy-start | bytes 1572868
  60.2 581.1 %all-to-all-start = ((bf16[8,8192,128]{2,0,1:T(8,128)(2,1)}), bf16[8,8192,128]{2,0,1:T(8,128)(2,1)}, u32[]{:S(2)}, u32[]{:S(2)}) async-start(bf16[8,8192,128]{2,0,1:T(8,128)(2,1)} %constant_dynamic-update-slice_fusion.1), calls=%async_computation | async-start | bytes 33554432 | tf_op jit(solution)/shard_map/all_to_all | solution.py:13
  77.7 845.6 %all-gather.2.cloned.1.call-start = ((), (), s32[]{:S(2)}) async-start(), calls=%async_computation.1 | async-start | bytes 2359296 | tf_op jit(solution)/shard_map/all_gather | solution.py:76
  82.0 574.3 %copy-start.4 = (s32[8]{0:T(128)S(1)}, s32[8]{0:T(128)}, u32[]{:S(2)}) copy-start(s32[8]{0:T(128)} %param.15) | copy-start | bytes 100
  801.4 0.7 copy-start.1
Sparse Core Ops, SparseCore 0:
  802.3 120.9 all-gather.1
